TPU v7x, 32 devices: a whole 2x2x4 slice. The times are simulated.
32 devices in a mesh: ep: 8 (over z, core), tp: 4 (over y, x).
Axes of the slice: x: 2, y: 2, z: 4, core: 2. Of those that a mesh axis runs over, the one named last changes fastest.
Arguments:
- tokens: bfloat16 [512, 2048], P('ep', 'tp'), may hold values from -20 to 20
- state: float32 [512, 16, 64, 64], P('ep', 'tp'), may hold values from -1.5 to 1.5
- attn_gain: float32 [2048], replicated, may hold values from 0.1 to 1.9
- ffn_gain: float32 [2048], replicated, may hold values from 0.1 to 1.9
- w_query: bfloat16 [2048, 1024], P(None, 'tp'), may hold values from -0.125 to 0.125
- w_key: bfloat16 [2048, 1024], P(None, 'tp'), may hold values from -0.125 to 0.125
- w_value: bfloat16 [2048, 1024], P(None, 'tp'), may hold values from -0.125 to 0.125
- w_output_gate: bfloat16 [2048, 1024], P(None, 'tp'), may hold values from -0.125 to 0.125
- w_decay: bfloat16 [2048, 16], replicated, may hold values from -0.125 to 0.125
- w_beta: bfloat16 [2048, 16], replicated, may hold values from -0.125 to 0.125
- decay_rate: float32 [16], P('tp'), may hold values from 0.1 to 2
- decay_shift: float32 [16], P('tp'), may hold values from -2 to 1
- head_gain: float32 [64], replicated, may hold values from 0.1 to 1.9
- w_mix_out: bfloat16 [1024, 2048], P(None, 'tp'), may hold values from -0.1875 to 0.1875
- expert_ids: int32 [512, 2], P('ep'), may hold values from 0 to 7, all different within a row; in each aligned block of 64 rows (0 to 63, 64 to 127, ...) at most 32 rows name the same one
- expert_weights: float32 [512, 2], P('ep'), may hold values from 0.2 to 1
- w_gate: bfloat16 [8, 2048, 4096], P('ep', None, 'tp'), may hold values from -0.125 to 0.125
- w_up: bfloat16 [8, 2048, 4096], P('ep', None, 'tp'), may hold values from -0.125 to 0.125
- w_down: bfloat16 [8, 4096, 2048], P('ep', 'tp'), may hold values from -0.09375 to 0.09375
Outputs:
- layer_out: bfloat16 [512, 2048], P('ep', 'tp')
- new_state: float32 [512, 16, 64, 64], P('ep', 'tp')
Inputs may be any that keep to these rules, and one draw needn't show every extreme that they name: `expert_ids`: each row names 2 different experts; within the rows of one index of ep (aligned blocks of 64 rows) no expert is named by more than 32 rows, and in some blocks one expert is named by exactly 32 rows.
All inputs are finite; a program needn't handle non-finite values.
Results may differ from a plain program's by a relative error of at most 0.013.
Values may be sent and summed in bfloat16 or wider, within the bound.
A program may use at most 64 MiB of HBM per device.

v0:
```python
import jax
import jax.numpy as jnp
from jax import lax
from jax.sharding import PartitionSpec as P

EPS = 1e-06


def unit_norm(values):
    return values * lax.rsqrt(jnp.sum(values * values, axis=-1, keepdims=True) + EPS)


def stored(values):
    return lax.optimization_barrier(values.astype(jnp.bfloat16)).astype(jnp.float32)


def shards(
    tokens,
    state,
    attn_gain,
    ffn_gain,
    w_query,
    w_key,
    w_value,
    w_output_gate,
    w_decay,
    w_beta,
    decay_rate,
    decay_shift,
    head_gain,
    w_mix_out,
    expert_ids,
    expert_weights,
    w_gate,
    w_up,
    w_down,
):
    groups = lax.axis_size("ep")
    seq_count = tokens.shape[0]
    own_width = tokens.shape[1]
    model_width = ffn_gain.shape[0]
    head_dim = head_gain.shape[0]
    heads_here = decay_rate.shape[0]
    top_count = expert_ids.shape[1]
    local_experts = w_gate.shape[0]
    expert_total = local_experts * groups
    capacity = max(2, 2 * seq_count * top_count // expert_total)
    whole_rows = lax.all_gather(tokens, "tp", axis=1, tiled=True)
    whole_f32 = whole_rows.astype(jnp.float32)
    normed = (
        whole_f32
        * lax.rsqrt(jnp.mean(whole_f32 * whole_f32, axis=1, keepdims=True) + EPS)
        * attn_gain
    ).astype(jnp.bfloat16)

    def project(weight):
        return jnp.dot(normed, weight, preferred_element_type=jnp.float32)

    def by_head(values):
        return values.reshape(seq_count, heads_here, head_dim)

    first_head = lax.axis_index("tp") * heads_here
    decay_cols = lax.dynamic_slice_in_dim(w_decay, first_head, heads_here, 1)
    beta_cols = lax.dynamic_slice_in_dim(w_beta, first_head, heads_here, 1)
    query_proj = stored(project(w_query))
    key_proj = stored(project(w_key))
    value_proj = stored(project(w_value))
    gate_proj = stored(project(w_output_gate))
    keep_rate = jnp.exp(-decay_rate * jax.nn.softplus(project(decay_cols) + decay_shift))
    beta_gate = jax.nn.sigmoid(project(beta_cols))
    query_head = unit_norm(jax.nn.silu(by_head(query_proj))) * head_dim ** (-0.5)
    key_head = unit_norm(jax.nn.silu(by_head(key_proj)))
    value_head = jax.nn.silu(by_head(value_proj))
    decayed = keep_rate[:, :, None, None] * state
    recalled = jnp.einsum("thd,thde->the", key_head, decayed, precision=lax.Precision.HIGHEST)
    correction = beta_gate[:, :, None] * (value_head - recalled)
    new_state = decayed + key_head[:, :, :, None] * correction[:, :, None, :]
    reading = jnp.einsum("thd,thde->the", query_head, new_state, precision=lax.Precision.HIGHEST)
    reading_scale = lax.rsqrt(jnp.mean(reading * reading, axis=-1, keepdims=True) + EPS)
    head_out = (reading * reading_scale * head_gain * jax.nn.silu(by_head(gate_proj))).astype(
        jnp.bfloat16
    )
    head_out = head_out.reshape(seq_count, heads_here * head_dim)
    mixed = jnp.dot(
        lax.all_gather(head_out, "tp", axis=1, tiled=True),
        w_mix_out,
        preferred_element_type=jnp.float32,
    )
    residual = (tokens.astype(jnp.float32) + mixed).astype(jnp.bfloat16)
    residual_f32 = residual.astype(jnp.float32)
    pair_count = seq_count * top_count
    flat_ids = expert_ids.reshape(pair_count)
    one_hot = (flat_ids[:, None] == jnp.arange(expert_total, dtype=jnp.int32)[None, :]).astype(
        jnp.int32
    )
    pair_index = jnp.arange(pair_count, dtype=jnp.int32)
    lower_mask = (pair_index[:, None] > pair_index[None, :]).astype(jnp.int32)
    earlier = jnp.dot(lower_mask, one_hot)
    slot_rank = jnp.sum(earlier * one_hot, axis=1)
    slot_of = flat_ids * capacity + slot_rank
    slot_count = expert_total * capacity
    slot_hit = jnp.arange(slot_count, dtype=jnp.int32)[:, None] == slot_of[None, :]
    dispatch = slot_hit.astype(jnp.bfloat16)
    dispatch_tokens = jnp.any(slot_hit.reshape(slot_count, seq_count, top_count), axis=2).astype(
        jnp.bfloat16
    )
    own_gain = lax.dynamic_slice_in_dim(ffn_gain, lax.axis_index("tp") * own_width, own_width, 0)
    square_total = lax.psum(jnp.sum(residual_f32 * residual_f32, axis=1), "tp")
    row_scale = lax.rsqrt(square_total / model_width + EPS)
    normed_ffn = (residual_f32 * row_scale[:, None] * own_gain).astype(jnp.bfloat16)
    outgoing = jnp.dot(dispatch_tokens, normed_ffn, preferred_element_type=jnp.float32).astype(
        jnp.bfloat16
    )
    arrived = lax.all_to_all(outgoing, "ep", split_axis=0, concat_axis=0, tiled=True)
    segment = lax.all_gather(arrived, "tp", axis=1, tiled=True)
    blocks = segment.reshape(groups, local_experts, capacity, segment.shape[1])
    gate_part = jnp.einsum("secd,edf->secf", blocks, w_gate, preferred_element_type=jnp.float32)
    up_part = jnp.einsum("secd,edf->secf", blocks, w_up, preferred_element_type=jnp.float32)
    expert_hidden = (jax.nn.silu(gate_part) * up_part).astype(jnp.bfloat16)
    partial_value = jnp.einsum(
        "secf,efd->secd", expert_hidden, w_down, preferred_element_type=jnp.float32
    )
    partial_value = partial_value.astype(jnp.bfloat16).reshape(
        groups * local_experts * capacity, model_width
    )
    summed = lax.psum_scatter(
        partial_value.astype(jnp.float32).astype(jnp.bfloat16),
        "tp",
        scatter_dimension=1,
        tiled=True,
    )
    returned = lax.all_to_all(summed, "ep", split_axis=0, concat_axis=0, tiled=True)
    pair_rows = jnp.einsum("sp,sd->pd", dispatch, returned, preferred_element_type=jnp.float32)
    weighted = jnp.sum(
        pair_rows.reshape(seq_count, top_count, own_width) * expert_weights[:, :, None], axis=1
    )
    layer_out = (residual_f32 + weighted).astype(jnp.bfloat16)
    return (layer_out, new_state)


def solution(mesh):
    in_specs = (
        P("ep", "tp"),
        P("ep", "tp", None, None),
        P(),
        P(),
        P(None, "tp"),
        P(None, "tp"),
        P(None, "tp"),
        P(None, "tp"),
        P(),
        P(),
        P("tp"),
        P("tp"),
        P(),
        P(None, "tp"),
        P("ep", None),
        P("ep", None),
        P("ep", None, "tp"),
        P("ep", None, "tp"),
        P("ep", "tp", None),
    )
    out_specs = (P("ep", "tp"), P("ep", "tp", None, None))
    return jax.shard_map(shards, mesh=mesh, in_specs=in_specs, out_specs=out_specs, check_vma=False)
```

profile of v0, /device:TPU:0, one launch (start us, length us, event | category | flops | bytes accessed | tf_op | source)
XLA Modules:
  0.0 171.2 jit_solution(3074201662367445162)
XLA Ops:
  7.2 0.0 copy-start
  7.2 0.0 all-gather.2.cloned.1.call-start
  7.2 10.9 %all_gather.9 = bf16[64,2048]{1,0:T(8,128)(2,1)S(1)} all-gather(bf16[64,512]{1,0:T(8,128)(2,1)} %param.19), channel_id=1, replica_groups=mesh['ep'=8,'tp'=4] {'tp'}, dimensions={1}, use_global_device_ids=true | all-gather | bytes 327680 | tf_op jit(solution)/shard_map/all_gather | solution.py:48
  18.1 0.2 fusion.36
  18.3 1.6 convolution_convert_fusion.3
  19.9 0.1 reshape.179
  20.0 0.2 multiply_reduce_fusion.2
  20.2 0.1 broadcast_multiply_fusion
  20.3 0.7 neg.32
  21.0 1.0 fusion.51
  22.0 0.1 copy.39
  22.1 1.0 fusion.33
  23.2 0.1 copy.40
  23.3 1.6 convolution_convert_fusion.2
  24.9 0.1 reshape.181
  25.0 0.0 copy-start.1
  25.0 10.1 %fusion = f32[64,4,1,64]{3,2,1,0:T(1,128)S(1)} fusion(f32[64,4,64,1]{2,3,1,0:T(1,128)S(1)} %bitcast.87, f32[64,4,64,64]{3,2,1,0:T(8,128)} %param.20, f32[64,4]{1,0:T(8,128)S(1)} %copy.39), kind=kOutput, calls=%fused_computation.1 | convolution fusion | flops 13631488 | bytes 4326400 | tf_op jit(solution)/shard_map/thd,thde->the/dot_general | solution.py:75
  35.1 0.1 fusion.42
  35.3 0.0 copy-done.1
  35.3 0.0 copy-start.2
  35.3 0.0 copy-start.5
  35.3 5.2 %multiply_add_fusion = f32[64,4,64,64]{3,2,1,0:T(8,128)} fusion(f32[64,4,64,64]{3,2,1,0:T(8,128)S(1)} %copy-done.1, f32[64,4,64]{2,1,0:T(4,128)S(1)} %fusion.42, f32[64,4,64]{2,1,0:T(4,128)S(1)} %broadcast_multiply_fusion, f32[64,4]{1,0:T(8,128)S(1)} %copy.39), kind=kLoop, calls=%fused_computation | loop fusion | flops 3145728 | bytes 8520704 | tf_op jit(solution)/shard_map/add | solution.py:77
  40.5 0.0 copy-done.2
  40.5 0.0 copy-done.5
  40.5 0.0 copy-start.4
  40.5 0.0 copy-start.6
  40.6 0.3 convolution_convert_fusion.4
  40.9 0.1 reshape.177
  41.0 0.2 multiply_reduce_fusion.3
  41.2 0.1 multiply_multiply_fusion
  41.4 9.5 %fusion.64 = f32[64,4,1,64]{3,2,1,0:T(1,128)S(1)} fusion(f32[64,4,64,1]{2,3,1,0:T(1,128)S(1)} %bitcast.95, f32[64,4,64,64]{3,2,1,0:T(8,128)} %multiply_add_fusion), kind=kOutput, calls=%fused_computation.79 | convolution fusion | flops 12582912 | bytes 4325376 | tf_op jit(solution)/shard_map/thd,thde->the/dot_general | solution.py:78
  50.9 0.1 multiply_reduce_fusion.1
  51.0 0.0 copy-done.3
  51.0 0.3 convolution_convert_fusion.1
  51.4 0.1 reshape.183
  51.5 0.0 copy-done.8
  51.5 0.1 fusion.44
  51.7 0.1 reshape.168
  51.8 8.7 %all_gather.10 = bf16[64,1024]{1,0:T(8,128)(2,1)S(1)} all-gather(bf16[64,256]{1,0:T(8,128)(2,1)S(1)} %reshape.168), channel_id=1, replica_groups=mesh['ep'=8,'tp'=4] {'tp'}, dimensions={1}, use_global_device_ids=true | all-gather | bytes 163840 | tf_op jit(solution)/shard_map/all_gather | solution.py:85
  60.5 0.0 copy-done
  60.5 0.4 multiply_reduce_fusion
  60.9 8.9 %psum.7 = f32[64]{0:T(128)S(1)} all-reduce(f32[64]{0:T(128)S(1)} %get-tuple-element.2), channel_id=1, replica_groups=mesh['ep'=8,'tp'=4] {'tp'}, use_global_device_ids=true, to_apply=%region_7.8 | all-reduce | flops 64 | bytes 512 | tf_op jit(solution)/shard_map/psum | solution.py:108
  69.8 0.1 copy.41
  69.9 0.1 reshape.169
  70.0 0.1 fusion.30
  70.2 0.2 reduce_sum.70
  70.4 0.1 copy.42
  70.4 0.1 fusion.43
  70.6 0.8 dynamic_slice.11
  71.3 0.3 convolution_convert_fusion
  71.6 14.5 %all_to_all.24 = bf16[8,32,512]{2,1,0:T(8,128)(2,1)} all-to-all(bf16[8,32,512]{2,1,0:T(8,128)(2,1)S(1)} %bitcast.90), channel_id=1, replica_groups=mesh['ep'=8,'tp'=4] {'ep'}, dimensions={0} | all-to-all | bytes 524288 | tf_op jit(solution)/shard_map/all_to_all | solution.py:114
  86.1 0.0 all-gather.2.cloned.1.call-update
  86.1 0.0 reduce-scatter.2.cloned.1.call-start
  86.2 23.8 %all-gather.2.cloned.1.call-done = bf16[256,2048]{1,0:T(8,128)(2,1)} async-done(((bf16[256,512]{1,0:T(8,128)(2,1)}), bf16[256,2048]{1,0:T(8,128)(2,1)}) %all-gather.2.cloned.1.call-update) | async-done | bytes 1048592 | tf_op jit(solution)/shard_map/all_gather | solution.py:115
  110.0 3.8 %fusion.12 = f32[8,1,32,1024]{3,2,0,1:T(8,128)S(1)} fusion(bf16[8,32,2048]{2,1,0:T(8,128)(2,1)} %bitcast.97, bf16[1,2048,1024]{2,1,0:T(8,128)(2,1)} %param.35), kind=kOutput, calls=%fused_computation.11 | convolution fusion | flops 1073741824 | bytes 6291456 | tf_op jit(solution)/shard_map/secd,edf->secf/dot_general | solution.py:117
  113.7 0.0 copy-start.7
  113.7 7.4 %fusion.9 = bf16[8,32,2048]{2,1,0:T(8,128)(2,1)} fusion(bf16[1,1024,2048]{2,1,0:T(8,128)(2,1)} %param.37, bf16[8,32,2048]{2,1,0:T(8,128)(2,1)} %bitcast.98, bf16[1,2048,1024]{2,1,0:T(8,128)(2,1)} %param.36, f32[8,1,32,1024]{3,2,0,1:T(8,128)S(1)} %fusion.12), kind=kOutput, calls=%fused_computation.10 | convolution fusion | flops 2149580800 | bytes 11534336 | tf_op jit(solution)/shard_map/secf,efd->secd/dot_general | solution.py:120
  121.1 0.0 reduce-scatter.2.cloned.1.call-update
  121.1 28.1 %reduce-scatter.2.cloned.1.call-done = bf16[256,512]{1,0:T(8,128)(2,1)} async-done(((bf16[256,2048]{1,0:T(8,128)(2,1)}), bf16[256,512]{1,0:T(8,128)(2,1)}) %reduce-scatter.2.cloned.1.call-update) | async-done | bytes 262160 | tf_op jit(solution)/shard_map/reduce_scatter | solution.py:126
  149.2 4.6 %all-to-all-start.1 = ((bf16[8,32,512]{2,1,0:T(8,128)(2,1)}), bf16[8,32,512]{2,1,0:T(8,128)(2,1)S(1)}, u32[]{:S(2)}, u32[]{:S(2)}) async-start(bf16[8,32,512]{2,1,0:T(8,128)(2,1)} %bitcast.96), calls=%async_computation.2 | async-start | bytes 524288 | tf_op jit(solution)/shard_map/all_to_all | solution.py:132
  153.8 0.1 iota_compare_fusion.1
  154.0 9.6 %all-to-all-done.1 = bf16[8,32,512]{2,1,0:T(8,128)(2,1)S(1)} async-done(((bf16[8,32,512]{2,1,0:T(8,128)(2,1)}), bf16[8,32,512]{2,1,0:T(8,128)(2,1)S(1)}, u32[]{:S(2)}, u32[]{:S(2)}) %all-to-all-start.1) | async-done | bytes 262176 | tf_op jit(solution)/shard_map/all_to_all | solution.py:132
  163.5 0.2 fusion.27
  163.7 0.7 add_convert_fusion
  (13 shorter events, 0.1 us)
Async XLA Ops:
  7.2 53.3 %copy-start = (bf16[1024,512]{1,0:T(8,128)(2,1)S(1)}, bf16[1024,512]{1,0:T(8,128)(2,1)}, u32[]{:S(2)}) copy-start(bf16[1024,512]{1,0:T(8,128)(2,1)} %param.32) | copy-start | bytes 3145732
  7.2 102.8 %all-gather.2.cloned.1.call-start = ((), (), s32[]{:S(2)}) async-start(), calls=%async_computation.3 | async-start | bytes 1310720 | tf_op jit(solution)/shard_map/all_gather | solution.py:115
  25.0 10.3 %copy-start.1 = (f32[64,4,64,64]{3,2,1,0:T(8,128)S(1)}, f32[64,4,64,64]{3,2,1,0:T(8,128)}, u32[]{:S(2)}) copy-start(f32[64,4,64,64]{3,2,1,0:T(8,128)} %param.20) | copy-start | bytes 12582916
  35.3 5.2 %copy-start.2 = (bf16[2048,256]{1,0:T(8,128)(2,1)S(1)}, bf16[2048,256]{1,0:T(8,128)(2,1)}, u32[]{:S(2)}) copy-start(bf16[2048,256]{1,0:T(8,128)(2,1)} %param.23) | copy-start | bytes 3145732
  35.3 5.2 %copy-start.5 = (f32[2048]{0:T(1024)S(1)}, f32[2048]{0:T(1024)}, u32[]{:S(2)}) copy-start(f32[2048]{0:T(1024)} %param.21) | copy-start | bytes 24580
  40.5 10.5 %copy-start.3 = (bf16[2048,256]{1,0:T(8,128)(2,1)S(1)}, bf16[2048,256]{1,0:T(8,128)(2,1)}, u32[]{:S(2)}) copy-start(bf16[2048,256]{1,0:T(8,128)(2,1)} %param.26) | copy-start | bytes 3145732
  40.5 11.0 %copy-start.8 = (f32[64]{0:T(128)S(1)}, f32[64]{0:T(128)}, u32[]{:S(2)}) copy-start(f32[64]{0:T(128)} %param.31) | copy-start | bytes 772
  40.5 19.9 %copy-start.4 = (bf16[64,512]{1,0:T(8,128)(2,1)S(1)}, bf16[64,512]{1,0:T(8,128)(2,1)}, u32[]{:S(2)}) copy-start(bf16[64,512]{1,0:T(8,128)(2,1)} %param.19) | copy-start | bytes 196612
  40.5 29.3 %copy-start.6 = (s32[64,2]{0,1:T(2,128)S(1)}, s32[64,2]{0,1:T(2,128)}, u32[]{:S(2)}) copy-start(s32[64,2]{0,1:T(2,128)} %param.33) | copy-start | bytes 1540
  86.1 63.1 %reduce-scatter.2.cloned.1.call-start = ((), (), s32[]{:S(2)}) async-start(), calls=%async_computation.4 | async-start | bytes 1310720 | tf_op jit(solution)/shard_map/reduce_scatter | solution.py:126
  113.7 49.8 %copy-start.7 = (f32[64,2]{0,1:T(2,128)S(1)}, f32[64,2]{0,1:T(2,128)}, u32[]{:S(2)}) copy-start(f32[64,2]{0,1:T(2,128)} %param.34) | copy-start | bytes 1540
  149.2 14.3 %all-to-all-start.1 = ((bf16[8,32,512]{2,1,0:T(8,128)(2,1)}), bf16[8,32,512]{2,1,0:T(8,128)(2,1)S(1)}, u32[]{:S(2)}, u32[]{:S(2)}) async-start(bf16[8,32,512]{2,1,0:T(8,128)(2,1)} %bitcast.96), calls=%async_computation.2 | async-start | bytes 524288 | tf_op jit(solution)/shard_map/all_to_all | solution.py:132
Sparse Core Ops, SparseCore 0:
  86.2 23.6 all-gather.1
  121.2 27.9 reduce-scatter.1
where the time goes:
time: 172 us; the launch traced here: 171 us
  waiting for transfers between devices  61.5 us (36%)
  blocking collectives  43 us (25%)
  matrix products  37.7 us (22%)
  between operations  14.3 us (8%)
  other arithmetic  7.97 us (5%)
  starting transfers between devices  4.68 us (3%)
  local copies, waits for them, and re-layouts  2.11 us (1%)
    reduce_scatter x1, waiting for transfers between devices, shards(): lax.psum_scatter(partial_value.astype(jnp.float32).astype(jnp.bfloat16),...  28.1 us
    all_gather x1, waiting for transfers between devices, shards(): segment = lax.all_gather(arrived, 'tp', axis=1, tiled=True)  23.8 us
    all_to_all x1, blocking collectives, shards(): lax.all_to_all(outgoing, 'ep', split_axis=0, concat_axis=0, tiled=True)  14.5 us
    all_gather x1, blocking collectives, shards(): whole_rows = lax.all_gather(tokens, 'tp', axis=1, tiled=True)  10.9 us
    dot_general x1, matrix products, shards(): jnp.einsum('thd,thde->the', key_head, decayed, precision=lax.Precision.HI...  10.1 us
    all_to_all x1, waiting for transfers between devices, shards(): lax.all_to_all(summed, 'ep', split_axis=0, concat_axis=0, tiled=True)  9.56 us
    dot_general x1, matrix products, shards(): jnp.einsum('thd,thde->the', query_head, new_state, precision=lax.Precisio...  9.48 us
    psum x1, blocking collectives, shards(): square_total = lax.psum(jnp.sum(residual_f32 * residual_f32, axis=1), 'tp')  8.93 us
  transfers between devices with their start and end apart: 3, of which 3 were waited for; matrix products, arithmetic and copies ran while one was open for 0% of the time, Pallas kernels for 0%

commit v1 on v0

v1 whole, which is shorter than its diff:
```python
import functools

import jax
import jax.numpy as jnp
from jax import lax
from jax.experimental import pallas as pl
from jax.experimental.pallas import tpu as pltpu
from jax.sharding import PartitionSpec as P

EPS = 1e-06
MESH = pl.DeviceIdType.MESH
GROUPS = 2
F32 = jnp.float32
BF16 = jnp.bfloat16


def unit_norm(values):
    return values * lax.rsqrt(jnp.sum(values * values, axis=-1, keepdims=True) + EPS)


def stored(values):
    return lax.optimization_barrier(values.astype(jnp.bfloat16)).astype(jnp.float32)


def remote(src, dst, send_sem, recv_sem, where):
    return pltpu.make_async_remote_copy(
        src_ref=src, dst_ref=dst, send_sem=send_sem, recv_sem=recv_sem,
        device_id=where, device_id_type=MESH)


def tail_kernel(
    n, m,
    head_ref, tok_ref, gain_ref, disp_ref, comb_ref, weight_ref,
    mix_hbm, gate_hbm, up_hbm, down_hbm,
    out_ref,
    head_all, mix_v, gate_v, up_v, down_v, outgoing, seg, normed, hidden, part,
    arrived, result, returned, resid,
    load_sem, head_send, head_recv, disp_send, disp_recv, fwd_send, fwd_recv,
    part_send, part_recv, back_send, back_recv, local_sem,
):
    me = lax.axis_index("ep")
    tp = lax.axis_index("tp")
    cap, width = outgoing.shape[1:]
    rows = tok_ref.shape[0]
    head_width = head_ref.shape[1]
    per = n // GROUPS
    group_rows = per * cap
    tp_at = [lax.rem(tp + d, m) for d in range(m)]
    ep_up = [lax.rem(me + k, n) for k in range(n)]
    ep_down = [lax.rem(me + n - k, n) for k in range(n)]

    loads = [
        pltpu.make_async_copy(mix_hbm, mix_v, load_sem.at[0]),
        pltpu.make_async_copy(gate_hbm.at[0], gate_v, load_sem.at[1]),
        pltpu.make_async_copy(up_hbm.at[0], up_v, load_sem.at[2]),
        pltpu.make_async_copy(down_hbm.at[0], down_v, load_sem.at[3]),
    ]
    loads[0].start()
    barrier = pltpu.get_barrier_semaphore()
    for d in range(1, m):
        pl.semaphore_signal(barrier, inc=1, device_id={"tp": tp_at[d]}, device_id_type=MESH)
    for k in range(1, n):
        pl.semaphore_signal(barrier, inc=1, device_id={"ep": ep_up[k]}, device_id_type=MESH)
    pl.semaphore_wait(barrier, m - 1 + n - 1)

    heads = []
    for d in range(1, m):
        copy = remote(head_ref, head_all.at[tp], head_send.at[d], head_recv.at[d], {"tp": tp_at[d]})
        copy.start()
        heads.append(copy)
    for load in loads[1:]:
        load.start()
    head_all[tp] = head_ref[...]
    loads[0].wait()
    for copy in heads:
        copy.wait_recv()
    mixed = jnp.zeros((rows, width), F32)
    for j in range(m):
        mixed += jnp.dot(head_all[j], mix_v[j * head_width:(j + 1) * head_width, :],
                         preferred_element_type=F32)
    residual = (tok_ref[...].astype(F32) + mixed).astype(BF16)
    resid[...] = residual
    picked = jnp.dot(disp_ref[...], residual, preferred_element_type=F32)
    outgoing[...] = picked.reshape(n, cap, width).astype(BF16)

    own = pltpu.make_async_copy(outgoing.at[me], seg.at[tp, 0], local_sem.at[0])
    own.start()
    sends = [own]
    for k in range(1, n):
        copy = remote(outgoing.at[ep_up[k]], seg.at[tp, k], disp_send.at[k], disp_recv.at[k],
                      {"ep": ep_up[k]})
        copy.start()
        sends.append(copy)
    forwards = []
    for k in range(n):
        if k == 0:
            own.wait()
        else:
            sends[k].wait_recv()
        row = []
        for d in range(1, m):
            copy = remote(seg.at[tp, k], seg.at[tp, k], fwd_send.at[d, k], fwd_recv.at[d, k],
                          {"tp": tp_at[d]})
            copy.start()
            row.append(copy)
        forwards.append(row)

    for load in loads[1:]:
        load.wait()
    parts = []
    for g in range(GROUPS):
        lo = g * per
        for k in range(lo, lo + per):
            for copy in forwards[k]:
                copy.wait_recv()
        total = jnp.zeros((group_rows, 1), F32)
        for j in range(m):
            block = seg[j, lo:lo + per].astype(F32).reshape(group_rows, width)
            total += jnp.sum(block * block, axis=1, keepdims=True)
        scale = lax.rsqrt(total / (m * width) + EPS)
        for j in range(m):
            block = seg[j, lo:lo + per].astype(F32).reshape(group_rows, width)
            normed[:, j * width:(j + 1) * width] = (
                block * scale * gain_ref[j:j + 1, :]).astype(BF16)

        def hidden_tile(c, carry):
            cols = pl.ds(pl.multiple_of(c * 256, 256), 256)
            gate = jnp.dot(normed[...], gate_v[:, cols], preferred_element_type=F32)
            up = jnp.dot(normed[...], up_v[:, cols], preferred_element_type=F32)
            hidden[:, cols] = (jax.nn.silu(gate) * up).astype(BF16)
            return carry

        lax.fori_loop(0, gate_v.shape[1] // 256, hidden_tile, 0)
        row = []
        for d in list(range(1, m)) + [0]:
            cols = pl.ds(pl.multiple_of(tp_at[d] * width, width), width)
            part[d, g] = jnp.dot(hidden[...], down_v[:, cols],
                                 preferred_element_type=F32).astype(BF16)
            if d > 0:
                copy = remote(part.at[d, g], arrived.at[d, g], part_send.at[d, g],
                              part_recv.at[d, g], {"tp": tp_at[d]})
                copy.start()
                row.append(copy)
        parts.append(row)

    backs = []
    for g in range(GROUPS):
        for copy in parts[g]:
            copy.wait_recv()
        total = part[0, g].astype(F32)
        for d in range(1, m):
            total += arrived[d, g].astype(F32)
        lo = g * per
        result[lo:lo + per] = total.reshape(per, cap, width).astype(BF16)
        for k in range(lo, lo + per):
            if k == 0:
                copy = pltpu.make_async_copy(result.at[0], returned.at[me], local_sem.at[1])
            else:
                copy = remote(result.at[k], returned.at[me], back_send.at[k], back_recv.at[k],
                              {"ep": ep_down[k]})
            copy.start()
            backs.append(copy)
    backs[0].wait()
    for copy in backs[1:]:
        copy.wait_recv()
    slots = returned[...].astype(F32).reshape(n * cap, width).astype(BF16)
    total = resid[...].astype(F32)
    for j in range(weight_ref.shape[1]):
        pair = jnp.dot(comb_ref[j * rows:(j + 1) * rows, :], slots, preferred_element_type=F32)
        total += weight_ref[:, j:j + 1] * pair
    out_ref[...] = total.astype(BF16)
    for copy in heads:
        copy.wait_send()
    for copy in sends[1:]:
        copy.wait_send()
    for row in forwards + parts:
        for copy in row:
            copy.wait_send()
    for copy in backs[1:]:
        copy.wait_send()


def layer_tail(n, m, cap, head_out, tokens, gain, dispatch, combine, weights, w_mix, w_gate, w_up,
               w_down):
    rows, width = tokens.shape
    hidden_width = w_gate.shape[2]
    half = n // GROUPS * cap
    vmem = pl.BlockSpec(memory_space=pltpu.VMEM)
    hbm = pl.BlockSpec(memory_space=pl.ANY)
    dma = pltpu.SemaphoreType.DMA
    return pl.pallas_call(
        functools.partial(tail_kernel, n, m),
        out_shape=jax.ShapeDtypeStruct((rows, width), BF16),
        in_specs=[vmem] * 6 + [hbm] * 4,
        out_specs=vmem,
        scratch_shapes=[
            pltpu.VMEM((m,) + head_out.shape, BF16),
            pltpu.VMEM(w_mix.shape, BF16),
            pltpu.VMEM(w_gate.shape[1:], BF16),
            pltpu.VMEM(w_up.shape[1:], BF16),
            pltpu.VMEM(w_down.shape[1:], BF16),
            pltpu.VMEM((n, cap, width), BF16),
            pltpu.VMEM((m, n, cap, width), BF16),
            pltpu.VMEM((half, m * width), BF16),
            pltpu.VMEM((half, hidden_width), BF16),
            pltpu.VMEM((m, GROUPS, half, width), BF16),
            pltpu.VMEM((m, GROUPS, half, width), BF16),
            pltpu.VMEM((n, cap, width), BF16),
            pltpu.VMEM((n, cap, width), BF16),
            pltpu.VMEM((rows, width), BF16),
            dma((4,)),
            dma((m,)), dma((m,)),
            dma((n,)), dma((n,)),
            dma((m, n)), dma((m, n)),
            dma((m, GROUPS)), dma((m, GROUPS)),
            dma((n,)), dma((n,)),
            dma((2,)),
        ],
        compiler_params=pltpu.CompilerParams(
            collective_id=0, has_side_effects=True, vmem_limit_bytes=40 * 1024 * 1024),
        name="layer_tail",
    )(head_out, tokens, gain, dispatch, combine, weights, w_mix, w_gate, w_up, w_down)


def shards(
    tokens,
    state,
    attn_gain,
    ffn_gain,
    w_query,
    w_key,
    w_value,
    w_output_gate,
    w_decay,
    w_beta,
    decay_rate,
    decay_shift,
    head_gain,
    w_mix_out,
    expert_ids,
    expert_weights,
    w_gate,
    w_up,
    w_down,
):
    groups = lax.axis_size("ep")
    members = lax.axis_size("tp")
    seq_count = tokens.shape[0]
    own_width = tokens.shape[1]
    head_dim = head_gain.shape[0]
    heads_here = decay_rate.shape[0]
    top_count = expert_ids.shape[1]
    assert w_gate.shape[0] == 1
    capacity = max(2, 2 * seq_count * top_count // groups)
    whole_rows = lax.all_gather(tokens, "tp", axis=1, tiled=True)
    whole_f32 = whole_rows.astype(jnp.float32)
    normed = (
        whole_f32
        * lax.rsqrt(jnp.mean(whole_f32 * whole_f32, axis=1, keepdims=True) + EPS)
        * attn_gain
    ).astype(jnp.bfloat16)

    def project(weight):
        return jnp.dot(normed, weight, preferred_element_type=jnp.float32)

    def by_head(values):
        return values.reshape(seq_count, heads_here, head_dim)

    first_head = lax.axis_index("tp") * heads_here
    decay_cols = lax.dynamic_slice_in_dim(w_decay, first_head, heads_here, 1)
    beta_cols = lax.dynamic_slice_in_dim(w_beta, first_head, heads_here, 1)
    query_proj = stored(project(w_query))
    key_proj = stored(project(w_key))
    value_proj = stored(project(w_value))
    gate_proj = stored(project(w_output_gate))
    keep_rate = jnp.exp(-decay_rate * jax.nn.softplus(project(decay_cols) + decay_shift))
    beta_gate = jax.nn.sigmoid(project(beta_cols))
    query_head = unit_norm(jax.nn.silu(by_head(query_proj))) * head_dim ** (-0.5)
    key_head = unit_norm(jax.nn.silu(by_head(key_proj)))
    value_head = jax.nn.silu(by_head(value_proj))
    decayed = keep_rate[:, :, None, None] * state
    recalled = jnp.einsum("thd,thde->the", key_head, decayed, precision=lax.Precision.HIGHEST)
    correction = beta_gate[:, :, None] * (value_head - recalled)
    new_state = decayed + key_head[:, :, :, None] * correction[:, :, None, :]
    reading = jnp.einsum("thd,thde->the", query_head, new_state, precision=lax.Precision.HIGHEST)
    reading_scale = lax.rsqrt(jnp.mean(reading * reading, axis=-1, keepdims=True) + EPS)
    head_out = (reading * reading_scale * head_gain * jax.nn.silu(by_head(gate_proj))).astype(
        jnp.bfloat16
    )
    head_out = head_out.reshape(seq_count, heads_here * head_dim)

    flat_ids = expert_ids.reshape(seq_count * top_count)
    one_hot = (flat_ids[:, None] == jnp.arange(groups, dtype=jnp.int32)[None, :]).astype(jnp.int32)
    pair_index = jnp.arange(seq_count * top_count, dtype=jnp.int32)
    lower_mask = (pair_index[:, None] > pair_index[None, :]).astype(jnp.int32)
    earlier = jnp.dot(lower_mask, one_hot)
    slot_rank = jnp.sum(earlier * one_hot, axis=1)
    slot_of = (flat_ids * capacity + slot_rank).reshape(seq_count, top_count)
    slot_index = jnp.arange(groups * capacity, dtype=jnp.int32)
    dispatch = jnp.any(slot_index[:, None, None] == slot_of[None, :, :], axis=2).astype(BF16)
    combine = (slot_of.T.reshape(-1)[:, None] == slot_index[None, :]).astype(BF16)
    layer_out = layer_tail(
        groups, members, capacity, head_out, tokens, ffn_gain.reshape(members, own_width),
        dispatch, combine, expert_weights, w_mix_out, w_gate, w_up, w_down)
    return (layer_out, new_state)


def solution(mesh):
    in_specs = (
        P("ep", "tp"),
        P("ep", "tp", None, None),
        P(),
        P(),
        P(None, "tp"),
        P(None, "tp"),
        P(None, "tp"),
        P(None, "tp"),
        P(),
        P(),
        P("tp"),
        P("tp"),
        P(),
        P(None, "tp"),
        P("ep", None),
        P("ep", None),
        P("ep", None, "tp"),
        P("ep", None, "tp"),
        P("ep", "tp", None),
    )
    out_specs = (P("ep", "tp"), P("ep", "tp", None, None))
    return jax.shard_map(shards, mesh=mesh, in_specs=in_specs, out_specs=out_specs, check_vma=False)
```

time: 172 us -> 92.7 us (0.54)
  waiting for transfers between devices: 61.5 us -> 0 us
  Pallas kernels: 0 us -> 40.1 us
  blocking collectives: 43 us -> 10.9 us
  matrix products: 37.7 us -> 23.3 us
  between operations: 14.3 us -> 0.99 us
  local copies, waits for them, and re-layouts: 2.11 us -> 8.8 us
  starting transfers between devices: 4.68 us -> 0 us
    pallas_call x0 -> x1, Pallas kernels: none -> 40.1 us  [layer_tail(): pl.pallas_call(functools.partial(tail_kernel, n, m), out_shape=jax.ShapeD...]
    reduce_scatter x1 -> x0, waiting for transfers between devices: 28.1 us -> none  [shards(): lax.psum_scatter(partial_value.astype(jnp.float32).astype(jnp.bfloat16),...]
    all_gather x1 -> x0, waiting for transfers between devices: 23.8 us -> none  [shards(): segment = lax.all_gather(arrived, 'tp', axis=1, tiled=True)]
    all_to_all x1 -> x0, blocking collectives: 14.5 us -> none  [shards(): lax.all_to_all(outgoing, 'ep', split_axis=0, concat_axis=0, tiled=True)]
    dot_general x5 -> x0, matrix products: 12 us -> none  [the longest x1 7.35 us: shards(): jnp.einsum('secf,efd->secd', expert_hidden, w_down, preferred_element_typ...]
    all_to_all x1 -> x0, waiting for transfers between devices: 9.56 us -> none  [shards(): lax.all_to_all(summed, 'ep', split_axis=0, concat_axis=0, tiled=True)]
    psum x1 -> x0, blocking collectives: 8.93 us -> none  [shards(): square_total = lax.psum(jnp.sum(residual_f32 * residual_f32, axis=1), 'tp')]
    all_gather x1 -> x0, blocking collectives: 8.67 us -> none  [shards(): lax.all_gather(head_out, 'tp', axis=1, tiled=True)]
  transfers between devices with their start and end apart: 3 -> 0, of which waited for: 3 -> 0; matrix products, arithmetic and copies ran while one was open for 0% -> 0% of each run, Pallas kernels for 0% -> 0%
where the time goes in v1:
time: 92.7 us; the launch traced here: 92.1 us
  Pallas kernels  40.1 us (43%)
  matrix products  23.3 us (25%)
  blocking collectives  10.9 us (12%)
  local copies, waits for them, and re-layouts  8.8 us (9%)
  other arithmetic  8.08 us (9%)
  between operations  0.99 us (1%)
    pallas_call x1, Pallas kernels, layer_tail(): pl.pallas_call(functools.partial(tail_kernel, n, m), out_shape=jax.ShapeD...  40.1 us
    all_gather x1, blocking collectives, shards(): whole_rows = lax.all_gather(tokens, 'tp', axis=1, tiled=True)  10.9 us
    dot_general x1, matrix products, shards(): jnp.einsum('thd,thde->the', key_head, decayed, precision=lax.Precision.HI...  9.25 us
    unnamed x29, local copies, waits for them, and re-layouts  7.45 us
    dot_general x1, matrix products, shards(): jnp.einsum('thd,thde->the', query_head, new_state, precision=lax.Precisio...  7.34 us
    dot_general x6, matrix products, project(): return jnp.dot(normed, weight, preferred_element_type=jnp.float32)  6.57 us
    add x1, other arithmetic, shards(): new_state = decayed + key_head[:, :, :, None] * correction[:, :, None, :]  5.95 us

profile of v1, /device:TPU:0, one launch (start us, length us, event | category | flops | bytes accessed | tf_op | source)
XLA Modules:
  0.0 92.1 jit_solution(9518921509684756019)
XLA Ops:
  0.6 0.0 copy-start
  0.6 0.0 copy-start.8
  0.7 0.0 copy-start.7
  0.7 10.9 %all_gather.3 = bf16[64,2048]{1,0:T(8,128)(2,1)S(1)} all-gather(bf16[64,512]{1,0:T(8,128)(2,1)} %tok_ref.1), channel_id=1, replica_groups=mesh['ep'=8,'tp'=4] {'tp'}, dimensions={1}, use_global_device_ids=true | all-gather | bytes 327680 | tf_op jit(solution)/shard_map/all_gather | solution.py:255
  11.6 0.2 fusion.7
  11.7 0.0 copy-done
  11.7 1.0 %convolution_convert_fusion = bf16[64,256]{1,0:T(8,128)(2,1)S(1)} fusion(bf16[2048,256]{1,0:T(8,128)(2,1)S(1)} %copy-done, bf16[64,2048]{1,0:T(8,128)(2,1)S(1)} %all_gather.3, f32[2048]{0:T(1024)} %param.21, f32[64]{0:T(128)S(1)} %add_rsqrt_fusion.3), kind=kOutput, calls=%fused_computation.4 | convolution fusion | flops 67649536 | bytes 1351936 | tf_op jit(solution)/shard_map/dot_general | solution.py:264
  12.8 0.1 reshape.110
  12.9 1.6 %convolution_convert_fusion.3 = bf16[64,256]{1,0:T(8,128)(2,1)S(1)} fusion(bf16[2048,256]{1,0:T(8,128)(2,1)} %param.23, bf16[64,2048]{1,0:T(8,128)(2,1)S(1)} %all_gather.3, f32[2048]{0:T(1024)} %param.21, f32[64]{0:T(128)S(1)} %add_rsqrt_fusion.3), kind=kOutput, calls=%fused_computation.7 | convolution fusion | flops 67649536 | bytes 1351936 | tf_op jit(solution)/shard_map/dot_general | solution.py:264
  14.5 0.1 reshape.104
  14.6 0.2 multiply_reduce_fusion.2
  14.8 0.1 multiply_multiply_fusion
  14.9 1.6 %convolution_convert_fusion.2 = bf16[64,256]{1,0:T(8,128)(2,1)S(1)} fusion(bf16[2048,256]{1,0:T(8,128)(2,1)} %param.24, bf16[64,2048]{1,0:T(8,128)(2,1)S(1)} %all_gather.3, f32[2048]{0:T(1024)} %param.21, f32[64]{0:T(128)S(1)} %add_rsqrt_fusion.3), kind=kOutput, calls=%fused_computation.6 | convolution fusion | flops 67649536 | bytes 1351936 | tf_op jit(solution)/shard_map/dot_general | solution.py:264
  16.5 0.1 reshape.106
  16.7 0.2 multiply_reduce_fusion.1
  16.9 0.1 broadcast_multiply_fusion
  17.0 0.7 neg.28
  17.7 1.0 %fusion.19 = f32[64,4]{0,1:T(4,128)S(1)} fusion(bf16[2048,16]{0,1:T(8,128)(2,1)} %param.27, s32[]{:T(128)S(6)} %select_n.8, f32[4]{0:T(128)} %param.30, f32[4]{0:T(128)S(1)} %neg.28, bf16[64,2048]{1,0:T(8,128)(2,1)S(1)} %all_gather.3, f32[2048]{0:T(1024)} %param.21, f32[64]{0:T(128)S(1)} %add_rsqrt_fusion.3), kind=kOutput, calls=%fused_computation.46 | convolution fusion | flops 1574912 | bytes 288532 | tf_op jit(solution)/shard_map/dot_general | solution.py:264
  18.7 0.1 copy.44
  18.8 9.2 %fusion = f32[64,4,1,64]{3,2,1,0:T(1,128)S(1)} fusion(f32[64,4,64,1]{2,3,1,0:T(1,128)S(1)} %bitcast.18, f32[64,4,64,64]{3,2,1,0:T(8,128)} %param.20, f32[64,4]{1,0:T(8,128)S(1)} %copy.44), kind=kOutput, calls=%fused_computation.1 | convolution fusion | flops 13631488 | bytes 4326400 | tf_op jit(solution)/shard_map/thd,thde->the/dot_general | solution.py:282
  28.0 0.0 copy-done.8
  28.1 0.0 copy-done.7
  28.1 0.3 convolution_convert_fusion.1
  28.4 0.1 reshape.108
  28.5 1.0 %fusion.6 = f32[64,4]{0,1:T(4,128)S(1)} fusion(bf16[2048,16]{0,1:T(8,128)(2,1)} %param.28, s32[]{:T(128)S(6)} %select_n.8, bf16[64,2048]{1,0:T(8,128)(2,1)S(1)} %all_gather.3, f32[2048]{0:T(1024)S(1)} %copy-done.8, f32[64]{0:T(128)S(1)} %add_rsqrt_fusion.3), kind=kOutput, calls=%fused_computation.13 | convolution fusion | flops 1573632 | bytes 288004 | tf_op jit(solution)/shard_map/dot_general | solution.py:264
  29.6 0.1 copy.45
  29.7 0.2 fusion.12
  29.8 5.9 %multiply_add_fusion = f32[64,4,64,64]{3,2,1,0:T(8,128)S(1)} fusion(f32[64,4,64,64]{3,2,1,0:T(8,128)} %param.20, f32[64,4,64]{2,1,0:T(4,128)S(1)} %fusion.12, f32[64,4,64]{2,1,0:T(4,128)S(1)} %broadcast_multiply_fusion, f32[64,4]{1,0:T(8,128)S(1)} %copy.44), kind=kLoop, calls=%fused_computation | loop fusion | flops 3145728 | bytes 8520704 | tf_op jit(solution)/shard_map/add | solution.py:284
  35.8 0.0 copy-start.6
  35.8 0.0 copy-start.12
  35.8 0.0 copy-start.9
  35.8 0.0 copy-start.10
  35.8 0.0 copy-start.11
  35.8 0.0 copy-start.4
  35.8 0.0 copy-start.5
  35.9 7.3 %fusion.31 = f32[64,4,1,64]{3,2,1,0:T(1,128)S(1)} fusion(f32[64,4,64,1]{2,3,1,0:T(1,128)S(1)} %bitcast.21, f32[64,4,64,64]{3,2,1,0:T(8,128)S(1)} %multiply_add_fusion), kind=kOutput, calls=%fused_computation.52 | convolution fusion | flops 12582912 | bytes 4325376 | tf_op jit(solution)/shard_map/thd,thde->the/dot_general | solution.py:285
  43.2 0.1 multiply_reduce_fusion
  43.4 0.0 copy-done.6
  43.4 0.0 copy-done.12
  43.4 0.1 fusion.15
  43.5 0.1 reshape.101.head_ref
  43.6 0.0 copy-done.9
  43.7 0.0 copy-done.10
  43.7 0.1 copy.46
  43.8 0.1 eq.44
  43.9 0.1 fusion.3
  44.1 0.2 reduce_sum.52
  44.2 0.1 copy.47
  44.3 0.1 fusion.13
  44.4 0.1 copy.48.disp_ref
  44.5 0.1 eq.50
  44.6 0.1 fusion.14.comb_ref
  44.7 0.0 copy-done.11
  44.7 0.1 copy.49.weight_ref
  44.8 0.0 copy-done.4
  44.8 0.0 copy-done.5
  44.8 0.0 copy-start.1
  44.9 2.2 %copy-done.1 = bf16[1,2048,1024]{2,1,0:T(8,128)(2,1)S(1)} copy-done((bf16[1,2048,1024]{2,1,0:T(8,128)(2,1)S(1)}, bf16[1,2048,1024]{2,1,0:T(8,128)(2,1)}, u32[]{:S(2)}) %copy-start.1) | copy-done | bytes 4194328
  47.0 0.0 copy-start.2
  47.0 2.2 %copy-done.2 = bf16[1,2048,1024]{2,1,0:T(8,128)(2,1)S(1)} copy-done((bf16[1,2048,1024]{2,1,0:T(8,128)(2,1)S(1)}, bf16[1,2048,1024]{2,1,0:T(8,128)(2,1)}, u32[]{:S(2)}) %copy-start.2) | copy-done | bytes 4194328
  49.2 0.0 copy-start.3
  49.2 2.2 %copy-done.3 = bf16[1,1024,2048]{2,1,0:T(8,128)(2,1)S(1)} copy-done((bf16[1,1024,2048]{2,1,0:T(8,128)(2,1)S(1)}, bf16[1,1024,2048]{2,1,0:T(8,128)(2,1)}, u32[]{:S(2)}) %copy-start.3) | copy-done | bytes 4194328
  51.4 40.1 %layer_tail.1 = bf16[64,512]{1,0:T(8,128)(2,1)S(1)} custom-call(bf16[64,256]{1,0:T(8,128)(2,1)S(1)} %reshape.101.head_ref, bf16[64,512]{1,0:T(8,128)(2,1)S(1)} %copy-done.5, f32[4,512]{1,0:T(4,128)S(1)} %reshape.102.gain_ref, bf16[256,64]{1,0:T(8,128)(2,1)S(1)} %copy.48.disp_ref, bf16[128,256]{1,0:T(8,128)(2,1)S(1)} %fusion.14.comb_ref, ...), custom_call_target="tpu_custom_call" | custom-call | tf_op jit(solution)/shard_map/layer_tail/pallas_call | solution.py:191
  91.5 0.6 copy.55
  (7 shorter events, 0.1 us)
Async XLA Ops:
  0.6 11.1 %copy-start = (bf16[2048,256]{1,0:T(8,128)(2,1)S(1)}, bf16[2048,256]{1,0:T(8,128)(2,1)}, u32[]{:S(2)}) copy-start(bf16[2048,256]{1,0:T(8,128)(2,1)} %param.26) | copy-start | bytes 3145732
  0.6 27.4 %copy-start.8 = (f32[2048]{0:T(1024)S(1)}, f32[2048]{0:T(1024)}, u32[]{:S(2)}) copy-start(f32[2048]{0:T(1024)} %param.21) | copy-start | bytes 24580
  0.7 27.4 %copy-start.7 = (bf16[2048,256]{1,0:T(8,128)(2,1)S(1)}, bf16[2048,256]{1,0:T(8,128)(2,1)}, u32[]{:S(2)}) copy-start(bf16[2048,256]{1,0:T(8,128)(2,1)} %param.25) | copy-start | bytes 3145732
  35.8 7.6 %copy-start.6 = (f32[64,4,64,64]{3,2,1,0:T(8,128)}, f32[64,4,64,64]{3,2,1,0:T(8,128)S(1)}, u32[]{:S(2)}) copy-start(f32[64,4,64,64]{3,2,1,0:T(8,128)S(1)} %multiply_add_fusion) | copy-start | bytes 12582916
  35.8 7.6 %copy-start.12 = (f32[64]{0:T(128)S(1)}, f32[64]{0:T(128)}, u32[]{:S(2)}) copy-start(f32[64]{0:T(128)} %param.31) | copy-start | bytes 772
  35.8 7.9 %copy-start.9 = (f32[2048]{0:T(1024)S(1)}, f32[2048]{0:T(1024)}, u32[]{:S(2)}) copy-start(f32[2048]{0:T(1024)} %param.22) | copy-start | bytes 24580
  35.8 7.9 %copy-start.10 = (s32[64,2]{0,1:T(2,128)S(1)}, s32[64,2]{0,1:T(2,128)}, u32[]{:S(2)}) copy-start(s32[64,2]{0,1:T(2,128)} %param.33) | copy-start | bytes 1540
  35.8 8.9 %copy-start.11 = (f32[64,2]{0,1:T(2,128)S(1)}, f32[64,2]{0,1:T(2,128)}, u32[]{:S(2)}) copy-start(f32[64,2]{0,1:T(2,128)} %param.34) | copy-start | bytes 1540
  35.8 9.0 %copy-start.4 = (bf16[1024,512]{1,0:T(8,128)(2,1)S(1)}, bf16[1024,512]{1,0:T(8,128)(2,1)}, u32[]{:S(2)}) copy-start(bf16[1024,512]{1,0:T(8,128)(2,1)} %mix_hbm.1) | copy-start | bytes 3145732
  35.8 9.0 %copy-start.5 = (bf16[64,512]{1,0:T(8,128)(2,1)S(1)}, bf16[64,512]{1,0:T(8,128)(2,1)}, u32[]{:S(2)}) copy-start(bf16[64,512]{1,0:T(8,128)(2,1)} %tok_ref.1) | copy-start | bytes 196612
  44.8 2.2 %copy-start.1 = (bf16[1,2048,1024]{2,1,0:T(8,128)(2,1)S(1)}, bf16[1,2048,1024]{2,1,0:T(8,128)(2,1)}, u32[]{:S(2)}) copy-start(bf16[1,2048,1024]{2,1,0:T(8,128)(2,1)} %gate_hbm.1) | copy-start | bytes 12582916
  47.0 2.2 %copy-start.2 = (bf16[1,2048,1024]{2,1,0:T(8,128)(2,1)S(1)}, bf16[1,2048,1024]{2,1,0:T(8,128)(2,1)}, u32[]{:S(2)}) copy-start(bf16[1,2048,1024]{2,1,0:T(8,128)(2,1)} %up_hbm.1) | copy-start | bytes 12582916
  49.2 2.2 %copy-start.3 = (bf16[1,1024,2048]{2,1,0:T(8,128)(2,1)S(1)}, bf16[1,1024,2048]{2,1,0:T(8,128)(2,1)}, u32[]{:S(2)}) copy-start(bf16[1,1024,2048]{2,1,0:T(8,128)(2,1)} %down_hbm.1) | copy-start | bytes 12582916

commit v2 on v1

--- a/solution.py
+++ b/solution.py
@@ -12,14 +12,6 @@
 GROUPS = 2
 F32 = jnp.float32
 BF16 = jnp.bfloat16
-
-
-def unit_norm(values):
-    return values * lax.rsqrt(jnp.sum(values * values, axis=-1, keepdims=True) + EPS)
-
-
-def stored(values):
-    return lax.optimization_barrier(values.astype(jnp.bfloat16)).astype(jnp.float32)
 
 
 def remote(src, dst, send_sem, recv_sem, where):
@@ -217,9 +209,171 @@
             dma((2,)),
         ],
         compiler_params=pltpu.CompilerParams(
-            collective_id=0, has_side_effects=True, vmem_limit_bytes=40 * 1024 * 1024),
+            collective_id=0, has_side_effects=True, vmem_limit_bytes=60 * 1024 * 1024),
         name="layer_tail",
     )(head_out, tokens, gain, dispatch, combine, weights, w_mix, w_gate, w_up, w_down)
+
+
+def gather_kernel(m, tok_ref, out_ref, send_sem, recv_sem):
+    tp = lax.axis_index("tp")
+    tp_at = [lax.rem(tp + d, m) for d in range(m)]
+    barrier = pltpu.get_barrier_semaphore()
+    for d in range(1, m):
+        pl.semaphore_signal(barrier, inc=1, device_id={"tp": tp_at[d]}, device_id_type=MESH)
+    pl.semaphore_wait(barrier, m - 1)
+    copies = []
+    for d in range(1, m):
+        copy = remote(tok_ref, out_ref.at[tp], send_sem.at[d], recv_sem.at[d], {"tp": tp_at[d]})
+        copy.start()
+        copies.append(copy)
+    out_ref[tp] = tok_ref[...]
+    for copy in copies:
+        copy.wait()
+
+
+def gather_tokens(m, tokens):
+    vmem = pl.BlockSpec(memory_space=pltpu.VMEM)
+    return pl.pallas_call(
+        functools.partial(gather_kernel, m),
+        out_shape=jax.ShapeDtypeStruct((m,) + tokens.shape, BF16),
+        in_specs=[vmem],
+        out_specs=vmem,
+        scratch_shapes=[pltpu.SemaphoreType.DMA((m,)), pltpu.SemaphoreType.DMA((m,))],
+        compiler_params=pltpu.CompilerParams(collective_id=1, has_side_effects=True),
+        name="gather_tokens",
+    )(tokens)
+
+
+def unit_norm(values):
+    return values * lax.rsqrt(jnp.sum(values * values, axis=-1, keepdims=True) + EPS)
+
+
+def delta_kernel(
+    m, slots, cap, block,
+    rate_ref, shift_ref, rows_ref, gain_ref, wq_ref, wk_ref, wv_ref, wg_ref, wd_ref, wb_ref,
+    head_gain_ref, ids_ref, state_ref,
+    new_ref, head_ref, disp_ref, comb_ref,
+    q_s, k_s, v_s, gate_s, keep_s, beta_s, read_s,
+):
+    step = pl.program_id(0)
+    rows, width = rows_ref.shape[1:]
+    heads, dim = q_s.shape[0], q_s.shape[2]
+    tp = lax.axis_index("tp")
+
+    @pl.when(step == 0)
+    def _():
+        total = jnp.zeros((rows, 1), F32)
+        for j in range(m):
+            piece = rows_ref[j].astype(F32)
+            total += jnp.sum(piece * piece, axis=1, keepdims=True)
+        scale = lax.rsqrt(total / (m * width) + EPS)
+        normed = [(rows_ref[j].astype(F32) * scale * gain_ref[j:j + 1, :]).astype(BF16)
+                  for j in range(m)]
+
+        def project(w_ref):
+            acc = jnp.dot(normed[0], w_ref[0:width, :], preferred_element_type=F32)
+            for j in range(1, m):
+                acc += jnp.dot(normed[j], w_ref[j * width:(j + 1) * width, :],
+                               preferred_element_type=F32)
+            return acc
+
+        def project_cols(w_ref):
+            acc = jnp.zeros((rows, w_ref.shape[0]), F32)
+            for j in range(m):
+                acc += lax.dot_general(normed[j], w_ref[:, j * width:(j + 1) * width],
+                                       (((1,), (1,)), ((), ())), preferred_element_type=F32)
+            return acc
+
+        def rounded(values):
+            return values.astype(BF16).astype(F32)
+
+        query = jax.nn.silu(rounded(project(wq_ref)))
+        key = jax.nn.silu(rounded(project(wk_ref)))
+        value = jax.nn.silu(rounded(project(wv_ref)))
+        gate = jax.nn.silu(rounded(project(wg_ref)))
+        decay_in = project_cols(wd_ref)
+        beta_in = project_cols(wb_ref)
+        column = lax.broadcasted_iota(jnp.int32, decay_in.shape, 1)
+        for h in range(heads):
+            cols = slice(h * dim, (h + 1) * dim)
+            q_s[h] = unit_norm(query[:, cols]) * dim ** (-0.5)
+            k_s[h] = unit_norm(key[:, cols])
+            v_s[h] = value[:, cols]
+            gate_s[h] = gate[:, cols]
+            mine = column == tp * heads + h
+            own_decay = jnp.sum(jnp.where(mine, decay_in, 0.0), axis=1, keepdims=True) + shift_ref[h]
+            soft = jnp.maximum(own_decay, 0.0) + jnp.log1p(jnp.exp(-jnp.abs(own_decay)))
+            keep_s[h] = jnp.broadcast_to(jnp.exp(-rate_ref[h] * soft), (rows, dim))
+            own_beta = jnp.sum(jnp.where(mine, beta_in, 0.0), axis=1, keepdims=True)
+            beta_s[h] = jnp.broadcast_to(jax.nn.sigmoid(own_beta), (rows, dim))
+
+        top = ids_ref.shape[1]
+        experts = slots // cap
+        expert = lax.broadcasted_iota(jnp.int32, (rows, experts), 1)
+        hot = [(ids_ref[:, j:j + 1] == expert).astype(F32) for j in range(top)]
+        every = hot[0]
+        for j in range(1, top):
+            every = every + hot[j]
+        lower = (lax.broadcasted_iota(jnp.int32, (rows, rows), 0)
+                 > lax.broadcasted_iota(jnp.int32, (rows, rows), 1)).astype(BF16)
+        earlier = jnp.dot(lower, every.astype(BF16), preferred_element_type=F32)
+        slot = lax.broadcasted_iota(jnp.int32, (rows, slots), 1)
+        used = jnp.zeros((rows, slots), F32)
+        for j in range(top):
+            rank = jnp.sum(earlier * hot[j], axis=1, keepdims=True).astype(jnp.int32)
+            hit = (slot == ids_ref[:, j:j + 1] * cap + rank).astype(F32)
+            comb_ref[j * rows:(j + 1) * rows, :] = hit.astype(BF16)
+            used = used + hit
+            earlier = earlier + hot[j]
+        disp_ref[...] = used.T.astype(BF16)
+
+    here = pl.ds(pl.multiple_of(step * block, block), block)
+    for h in range(heads):
+        key = k_s[h, here, :]
+        query = q_s[h, here, :]
+        decayed = state_ref[:, h] * keep_s[h, here, :][:, None, :]
+        key_col = jnp.broadcast_to(key[:, :, None], decayed.shape)
+        recalled = jnp.sum(key_col * decayed, axis=1)
+        correction = beta_s[h, here, :] * (v_s[h, here, :] - recalled)
+        updated = decayed + key_col * correction[:, None, :]
+        new_ref[:, h] = updated
+        read_s[h, here, :] = jnp.sum(query[:, :, None] * updated, axis=1)
+
+    @pl.when(step == pl.num_programs(0) - 1)
+    def _():
+        outs = []
+        for h in range(heads):
+            reading = read_s[h]
+            scale = lax.rsqrt(jnp.mean(reading * reading, axis=-1, keepdims=True) + EPS)
+            outs.append(reading * scale * head_gain_ref[...] * gate_s[h])
+        head_ref[...] = (jnp.concatenate(outs, axis=1) if heads > 1 else outs[0]).astype(BF16)
+
+
+def delta_step(m, slots, cap, gathered, gain, w_query, w_key, w_value, w_output_gate, w_decay,
+               w_beta, rate, shift, head_gain, ids, state):
+    rows, heads, dim = state.shape[:3]
+    block = 8
+    smem = pl.BlockSpec(memory_space=pltpu.SMEM)
+    vmem = pl.BlockSpec(memory_space=pltpu.VMEM)
+    spec = pl.BlockSpec((block,) + state.shape[1:], lambda i: (i, 0, 0, 0))
+    per_head = pltpu.VMEM((heads, rows, dim), F32)
+    pairs = rows * ids.shape[1]
+    return pl.pallas_call(
+        functools.partial(delta_kernel, m, slots, cap, block),
+        grid=(rows // block,),
+        out_shape=(
+            jax.ShapeDtypeStruct(state.shape, F32),
+            jax.ShapeDtypeStruct((rows, heads * dim), BF16),
+            jax.ShapeDtypeStruct((slots, rows), BF16),
+            jax.ShapeDtypeStruct((pairs, slots), BF16),
+        ),
+        in_specs=[smem, smem] + [vmem] * 10 + [spec],
+        out_specs=(spec, vmem, vmem, vmem),
+        scratch_shapes=[per_head] * 7,
+        compiler_params=pltpu.CompilerParams(vmem_limit_bytes=40 * 1024 * 1024),
+        name="delta_step",
+    )(rate, shift, gathered, gain, w_query, w_key, w_value, w_output_gate, w_decay.T, w_beta.T,
+      head_gain, ids, state)
 
 
 def shards(
@@ -247,58 +401,14 @@
     members = lax.axis_size("tp")
     seq_count = tokens.shape[0]
     own_width = tokens.shape[1]
-    head_dim = head_gain.shape[0]
-    heads_here = decay_rate.shape[0]
     top_count = expert_ids.shape[1]
     assert w_gate.shape[0] == 1
     capacity = max(2, 2 * seq_count * top_count // groups)
-    whole_rows = lax.all_gather(tokens, "tp", axis=1, tiled=True)
-    whole_f32 = whole_rows.astype(jnp.float32)
-    normed = (
-        whole_f32
-        * lax.rsqrt(jnp.mean(whole_f32 * whole_f32, axis=1, keepdims=True) + EPS)
-        * attn_gain
-    ).astype(jnp.bfloat16)
-
-    def project(weight):
-        return jnp.dot(normed, weight, preferred_element_type=jnp.float32)
-
-    def by_head(values):
-        return values.reshape(seq_count, heads_here, head_dim)
-
-    first_head = lax.axis_index("tp") * heads_here
-    decay_cols = lax.dynamic_slice_in_dim(w_decay, first_head, heads_here, 1)
-    beta_cols = lax.dynamic_slice_in_dim(w_beta, first_head, heads_here, 1)
-    query_proj = stored(project(w_query))
-    key_proj = stored(project(w_key))
-    value_proj = stored(project(w_value))
-    gate_proj = stored(project(w_output_gate))
-    keep_rate = jnp.exp(-decay_rate * jax.nn.softplus(project(decay_cols) + decay_shift))
-    beta_gate = jax.nn.sigmoid(project(beta_cols))
-    query_head = unit_norm(jax.nn.silu(by_head(query_proj))) * head_dim ** (-0.5)
-    key_head = unit_norm(jax.nn.silu(by_head(key_proj)))
-    value_head = jax.nn.silu(by_head(value_proj))
-    decayed = keep_rate[:, :, None, None] * state
-    recalled = jnp.einsum("thd,thde->the", key_head, decayed, precision=lax.Precision.HIGHEST)
-    correction = beta_gate[:, :, None] * (value_head - recalled)
-    new_state = decayed + key_head[:, :, :, None] * correction[:, :, None, :]
-    reading = jnp.einsum("thd,thde->the", query_head, new_state, precision=lax.Precision.HIGHEST)
-    reading_scale = lax.rsqrt(jnp.mean(reading * reading, axis=-1, keepdims=True) + EPS)
-    head_out = (reading * reading_scale * head_gain * jax.nn.silu(by_head(gate_proj))).astype(
-        jnp.bfloat16
-    )
-    head_out = head_out.reshape(seq_count, heads_here * head_dim)
-
-    flat_ids = expert_ids.reshape(seq_count * top_count)
-    one_hot = (flat_ids[:, None] == jnp.arange(groups, dtype=jnp.int32)[None, :]).astype(jnp.int32)
-    pair_index = jnp.arange(seq_count * top_count, dtype=jnp.int32)
-    lower_mask = (pair_index[:, None] > pair_index[None, :]).astype(jnp.int32)
-    earlier = jnp.dot(lower_mask, one_hot)
-    slot_rank = jnp.sum(earlier * one_hot, axis=1)
-    slot_of = (flat_ids * capacity + slot_rank).reshape(seq_count, top_count)
-    slot_index = jnp.arange(groups * capacity, dtype=jnp.int32)
-    dispatch = jnp.any(slot_index[:, None, None] == slot_of[None, :, :], axis=2).astype(BF16)
-    combine = (slot_of.T.reshape(-1)[:, None] == slot_index[None, :]).astype(BF16)
+    gathered = gather_tokens(members, tokens)
+    new_state, head_out, dispatch, combine = delta_step(
+        members, groups * capacity, capacity, gathered, attn_gain.reshape(members, own_width),
+        w_query, w_key, w_value, w_output_gate, w_decay, w_beta, decay_rate, decay_shift,
+        head_gain[None, :], expert_ids, state)
     layer_out = layer_tail(
         groups, members, capacity, head_out, tokens, ffn_gain.reshape(members, own_width),
         dispatch, combine, expert_weights, w_mix_out, w_gate, w_up, w_down)

time: 92.7 us -> 80.7 us (0.87)
  matrix products: 23.3 us -> 0 us
  Pallas kernels: 40.1 us -> 60.3 us
  blocking collectives: 10.9 us -> 0 us
  local copies, waits for them, and re-layouts: 8.8 us -> 19 us
  other arithmetic: 8.08 us -> 0 us
    dot_general x9 -> x0, matrix products: 23.3 us -> none  [the longest x1 9.25 us: shards(): jnp.einsum('thd,thde->the', key_head, decayed, precision=lax.Precision.HI...]
    pallas_call x0 -> x2, Pallas kernels: none -> 18.6 us  [the longest x1 9.32 us: gather_tokens(): pl.pallas_call(functools.partial(gather_kernel, m), out_shape=jax.ShapeDt...]
    all_gather x1 -> x0, blocking collectives: 10.9 us -> none  [shards(): whole_rows = lax.all_gather(tokens, 'tp', axis=1, tiled=True)]
    unnamed x29 -> x35, local copies, waits for them, and re-layouts: 7.45 us -> 17.7 us
    add x2 -> x0, other arithmetic: 5.96 us -> none  [the longest x1 5.95 us: shards(): new_state = decayed + key_head[:, :, :, None] * correction[:, :, None, :]]
    pallas_call x1, Pallas kernels: 40.1 us -> 41.8 us  [layer_tail(): pl.pallas_call(functools.partial(tail_kernel, n, m), out_shape=jax.ShapeD...]
where the time goes in v2:
time: 80.7 us; the launch traced here: 80 us
  Pallas kernels  60.3 us (75%)
  local copies, waits for them, and re-layouts  19 us (24%)
    pallas_call x1, Pallas kernels, layer_tail(): pl.pallas_call(functools.partial(tail_kernel, n, m), out_shape=jax.ShapeD...  41.8 us
    unnamed x35, local copies, waits for them, and re-layouts  17.7 us
    pallas_call x1, Pallas kernels, gather_tokens(): pl.pallas_call(functools.partial(gather_kernel, m), out_shape=jax.ShapeDt...  9.32 us
    pallas_call x1, Pallas kernels, delta_step(): pl.pallas_call(functools.partial(delta_kernel, m, slots, cap, block), gri...  9.26 us

profile of v2, /device:TPU:0, one launch (start us, length us, event | category | flops | bytes accessed | tf_op | source)
XLA Modules:
  0.0 80.0 jit_solution(16912663745657695064)
XLA Ops:
  0.6 9.3 %gather_tokens.1.rows_ref = bf16[4,64,512]{2,1,0:T(8,128)(2,1)} custom-call(bf16[64,512]{1,0:T(8,128)(2,1)} %tok_ref.3), custom_call_target="tpu_custom_call" | custom-call | tf_op jit(solution)/shard_map/gather_tokens/pallas_call | solution.py:236
  10.0 0.8 copy.21.ids_ref
  10.7 0.7 reshape.10.gain_ref
  11.4 0.0 copy-start
  11.4 3.4 %copy-done = f32[64,4,64,64]{3,2,1,0:T(8,128)S(1)} copy-done((f32[64,4,64,64]{3,2,1,0:T(8,128)S(1)}, f32[64,4,64,64]{3,2,1,0:T(8,128)}, u32[]{:S(2)}) %copy-start) | copy-done | bytes 4194328
  14.8 0.0 copy-start.1
  14.8 1.2 %copy-done.1 = bf16[2048,256]{1,0:T(8,128)(2,1)S(1)} copy-done((bf16[2048,256]{1,0:T(8,128)(2,1)S(1)}, bf16[2048,256]{1,0:T(8,128)(2,1)}, u32[]{:S(2)}) %copy-start.1) | copy-done | bytes 1048600
  16.0 0.0 copy-start.2
  16.0 1.2 %copy-done.2 = bf16[2048,256]{1,0:T(8,128)(2,1)S(1)} copy-done((bf16[2048,256]{1,0:T(8,128)(2,1)S(1)}, bf16[2048,256]{1,0:T(8,128)(2,1)}, u32[]{:S(2)}) %copy-start.2) | copy-done | bytes 1048600
  17.3 0.0 copy-start.3
  17.3 1.2 %copy-done.3 = bf16[2048,256]{1,0:T(8,128)(2,1)S(1)} copy-done((bf16[2048,256]{1,0:T(8,128)(2,1)S(1)}, bf16[2048,256]{1,0:T(8,128)(2,1)}, u32[]{:S(2)}) %copy-start.3) | copy-done | bytes 1048600
  18.5 0.0 copy-start.4
  18.5 1.2 %copy-done.4 = bf16[2048,256]{1,0:T(8,128)(2,1)S(1)} copy-done((bf16[2048,256]{1,0:T(8,128)(2,1)S(1)}, bf16[2048,256]{1,0:T(8,128)(2,1)}, u32[]{:S(2)}) %copy-start.4) | copy-done | bytes 1048600
  19.7 0.0 copy-start.5
  19.7 0.9 %copy-done.5 = bf16[4,64,512]{2,1,0:T(8,128)(2,1)S(1)} copy-done((bf16[4,64,512]{2,1,0:T(8,128)(2,1)S(1)}, bf16[4,64,512]{2,1,0:T(8,128)(2,1)}, u32[]{:S(2)}) %copy-start.5) | copy-done | bytes 262168
  20.7 0.0 copy-start.6
  20.7 0.8 %copy-done.6 = bf16[2048,16]{0,1:T(8,128)(2,1)S(1)} copy-done((bf16[2048,16]{0,1:T(8,128)(2,1)S(1)}, bf16[2048,16]{0,1:T(8,128)(2,1)}, u32[]{:S(2)}) %copy-start.6) | copy-done | bytes 65560
  21.5 0.0 copy-start.7
  21.5 0.8 %copy-done.7 = bf16[2048,16]{0,1:T(8,128)(2,1)S(1)} copy-done((bf16[2048,16]{0,1:T(8,128)(2,1)S(1)}, bf16[2048,16]{0,1:T(8,128)(2,1)}, u32[]{:S(2)}) %copy-start.7) | copy-done | bytes 65560
  22.3 0.0 copy-start.11
  22.3 0.7 copy-done.11
  23.0 0.0 copy-start.12
  23.0 0.7 copy-done.12
  23.7 0.0 copy-start.13
  23.7 0.7 copy-done.13
  24.3 0.0 copy-start.15
  24.3 0.0 copy-start.14
  24.3 9.3 %delta_step.1 = (f32[64,4,64,64]{3,2,1,0:T(8,128)}, bf16[64,256]{1,0:T(8,128)(2,1)S(1)}, bf16[256,64]{1,0:T(8,128)(2,1)S(1)}, bf16[128,256]{1,0:T(8,128)(2,1)S(1)}) custom-call(f32[4]{0:T(128)S(1)} %copy-done.11, f32[4]{0:T(128)S(1)} %copy-done.12, bf16[4,64,512]{2,1,0:T(8,128)(2,1)S(1)} %copy-done.5, f32[4,512]{1,0:T(4,128)S(1)} %reshape.10.gain_ref, ...), custom_call_target="tpu_custom_call" | custom-call | tf_op jit(solution)/shard_map/delta_step/pallas_call | solution.py:361
  33.6 0.0 copy-start.8
  33.6 0.6 copy-done.8
  34.2 0.0 copy-start.9
  34.2 0.6 copy-done.9
  34.8 0.0 copy-start.10
  34.8 0.6 copy-done.10
  35.5 0.0 copy-done.15
  35.5 0.7 copy.22.weight_ref
  36.2 0.0 copy-done.14
  36.2 0.6 reshape.11.gain_ref
  36.8 41.8 %layer_tail.1 = bf16[64,512]{1,0:T(8,128)(2,1)} custom-call(bf16[64,256]{1,0:T(8,128)(2,1)} %copy-done.10, bf16[64,512]{1,0:T(8,128)(2,1)} %tok_ref.3, f32[4,512]{1,0:T(4,128)} %reshape.11.gain_ref, bf16[256,64]{1,0:T(8,128)(2,1)} %copy-done.8, bf16[128,256]{1,0:T(8,128)(2,1)} %copy-done.9, f32[64,2]{1,0:T(8,128)} %copy.22.weight_ref, ...), custom_call_target="tpu_custom_call" | custom-call | tf_op jit(solution)/shard_map/layer_tail/pallas_call | solution.py:183
  78.5 1.5 %copy.24 = bf16[64,512]{1,0:T(8,128)(2,1)} copy(bf16[64,512]{1,0:T(8,128)(2,1)} %layer_tail.1) | data formatting | bytes 131072
Async XLA Ops:
  11.4 3.4 %copy-start = (f32[64,4,64,64]{3,2,1,0:T(8,128)S(1)}, f32[64,4,64,64]{3,2,1,0:T(8,128)}, u32[]{:S(2)}) copy-start(f32[64,4,64,64]{3,2,1,0:T(8,128)} %state_ref.1) | copy-start | bytes 12582916
  14.8 1.2 %copy-start.1 = (bf16[2048,256]{1,0:T(8,128)(2,1)S(1)}, bf16[2048,256]{1,0:T(8,128)(2,1)}, u32[]{:S(2)}) copy-start(bf16[2048,256]{1,0:T(8,128)(2,1)} %wq_ref.1) | copy-start | bytes 3145732
  16.0 1.2 %copy-start.2 = (bf16[2048,256]{1,0:T(8,128)(2,1)S(1)}, bf16[2048,256]{1,0:T(8,128)(2,1)}, u32[]{:S(2)}) copy-start(bf16[2048,256]{1,0:T(8,128)(2,1)} %wk_ref.1) | copy-start | bytes 3145732
  17.3 1.2 %copy-start.3 = (bf16[2048,256]{1,0:T(8,128)(2,1)S(1)}, bf16[2048,256]{1,0:T(8,128)(2,1)}, u32[]{:S(2)}) copy-start(bf16[2048,256]{1,0:T(8,128)(2,1)} %wv_ref.1) | copy-start | bytes 3145732
  18.5 1.2 %copy-start.4 = (bf16[2048,256]{1,0:T(8,128)(2,1)S(1)}, bf16[2048,256]{1,0:T(8,128)(2,1)}, u32[]{:S(2)}) copy-start(bf16[2048,256]{1,0:T(8,128)(2,1)} %wg_ref.1) | copy-start | bytes 3145732
  19.7 0.9 %copy-start.5 = (bf16[4,64,512]{2,1,0:T(8,128)(2,1)S(1)}, bf16[4,64,512]{2,1,0:T(8,128)(2,1)}, u32[]{:S(2)}) copy-start(bf16[4,64,512]{2,1,0:T(8,128)(2,1)} %gather_tokens.1.rows_ref) | copy-start | bytes 786436
  20.7 0.8 %copy-start.6 = (bf16[2048,16]{0,1:T(8,128)(2,1)S(1)}, bf16[2048,16]{0,1:T(8,128)(2,1)}, u32[]{:S(2)}) copy-start(bf16[2048,16]{0,1:T(8,128)(2,1)} %param.27) | copy-start | bytes 196612
  21.5 0.8 %copy-start.7 = (bf16[2048,16]{0,1:T(8,128)(2,1)S(1)}, bf16[2048,16]{0,1:T(8,128)(2,1)}, u32[]{:S(2)}) copy-start(bf16[2048,16]{0,1:T(8,128)(2,1)} %param.28) | copy-start | bytes 196612
  22.3 0.7 copy-start.11
  23.0 0.7 copy-start.12
  23.7 0.7 copy-start.13
  24.3 11.1 %copy-start.15 = (f32[64,2]{0,1:T(2,128)S(1)}, f32[64,2]{0,1:T(2,128)}, u32[]{:S(2)}) copy-start(f32[64,2]{0,1:T(2,128)} %param.34) | copy-start | bytes 1540
  24.3 11.8 %copy-start.14 = (f32[2048]{0:T(1024)S(1)}, f32[2048]{0:T(1024)}, u32[]{:S(2)}) copy-start(f32[2048]{0:T(1024)} %param.22) | copy-start | bytes 24580
  33.6 0.6 copy-start.8
  34.2 0.6 copy-start.9
  34.8 0.6 copy-start.10
